TPU v7x, 256 devices: a whole 4x4x8 slice. The times are simulated.
256 devices in a mesh: kv: 16 (over y, x), tp: 16 (over z, core).
Axes of the slice: x: 4, y: 4, z: 8, core: 2. Of those that a mesh axis runs over, the one named last changes fastest.
Arguments:
- tokens: bfloat16 [16, 2048], P(None, 'kv'), may hold values from -40 to 40
- lengths: int32 [16], replicated, may hold values from 1 to 16384, 77824 in all
- cache_keys: bfloat16 [16, 16384, 16, 128], P(None, 'kv', 'tp'), may hold values from -200 to 200
- cache_values: bfloat16 [16, 16384, 16, 128], P(None, 'kv', 'tp'), may hold values from -6 to 6
- lambdas: float32 [16], P('tp'), may hold values from 0.3 to 0.8
- head_gain: bfloat16 [128], replicated, may hold values from 0.099609375 to 1.8984375
- attn_gain: bfloat16 [2048], P('kv'), may hold values from 0.099609375 to 1.8984375
- w_query: bfloat16 [2048, 2048], P('kv', 'tp'), may hold values from -0.125 to 0.125
- w_key: bfloat16 [2048, 2048], P('kv', 'tp'), may hold values from -0.5 to 0.5
- w_value: bfloat16 [2048, 2048], P('kv', 'tp'), may hold values from -0.125 to 0.125
- w_out: bfloat16 [2048, 2048], P('tp', 'kv'), may hold values from -0.125 to 0.125
- first_gain: bfloat16 [2048], P('kv'), may hold values from 0.099609375 to 1.8984375
- first_gate: bfloat16 [2048, 5632], P('kv', 'tp'), may hold values from -0.125 to 0.125
- first_up: bfloat16 [2048, 5632], P('kv', 'tp'), may hold values from -0.125 to 0.125
- first_down: bfloat16 [5632, 2048], P('tp', 'kv'), may hold values from -0.078125 to 0.078125
- second_gain: bfloat16 [2048], P('kv'), may hold values from 0.099609375 to 1.8984375
- second_gate: bfloat16 [2048, 5632], P('kv', 'tp'), may hold values from -0.125 to 0.125
- second_up: bfloat16 [2048, 5632], P('kv', 'tp'), may hold values from -0.125 to 0.125
- second_down: bfloat16 [5632, 2048], P('tp', 'kv'), may hold values from -0.078125 to 0.078125
Outputs:
- stream_out: bfloat16 [16, 2048], P(None, 'kv')
Inputs may be any that keep to these rules, and one draw needn't show every extreme that they name: `lengths`: one sequence has exactly 16384 live positions.
All inputs are finite; a program needn't handle non-finite values.
Results may differ from a plain program's by a relative error of at most 0.02.
Values may be sent and summed in bfloat16 or wider, within the bound.
A program may use at most 64 MiB of HBM per device.

v0:
```python
import jax
import jax.numpy as jnp
from jax import lax
from jax.sharding import Mesh
from jax.sharding import PartitionSpec as P

D = 2048
DK = 64
DV = 128
KV = ("kv_0", "kv_1")


EPSILON = 1e-06
ROTARY_BASE = 10000.0
OUTPUT_KEEP = 0.8
MASKED_SCORE = -1e30


def one_axis_at_a_time(value, axes):
    for axis in axes:
        value = lax.psum(value, axis)
    return value


def copy_for_each(value, axis):
    copies = jnp.broadcast_to(value, (lax.axis_size(axis), *value.shape))
    return lax.all_to_all(copies, axis, split_axis=0, concat_axis=0, tiled=True)


def taken_together(value, axis):
    everything = copy_for_each(value, axis)
    return jnp.sum(everything, axis=0)


def together(arrays, axis):
    ravelled, at, finished = (jnp.concatenate([a.reshape(-1) for a in arrays]), 0, [])
    running = taken_together(ravelled, axis)
    for a in arrays:
        finished.append(running[at : at + a.size].reshape(a.shape))
        at += a.size
    return tuple(finished)


def all_in_one(value, axis):
    leaves = jax.tree.leaves(value)
    turns = sorted(range(len(leaves)), key=lambda k: -leaves[k].size)
    width = (1, *leaves[turns[0]].shape)[-1]
    lines = [
        jnp.pad(leaves[k].reshape(-1), (0, -leaves[k].size % width)).reshape(-1, width)
        for k in turns
    ]
    both, at, found = (copy_for_each(jnp.concatenate(lines), axis), 0, {})
    for k, line in zip(turns, lines):
        share = both[:, at : at + len(line)].reshape(len(both), -1)
        found[k] = share[:, : leaves[k].size].reshape(-1, *leaves[k].shape)
        at += len(line)
    numbers = iter(range(len(leaves)))
    return jax.tree.map(lambda _: found[next(numbers)], value)


def combined_pairwise(pieces, combine):
    while len(jax.tree.leaves(pieces)[0]) > 1:
        pieces = jax.vmap(combine)(
            *(jax.tree.map(lambda part: part[side::2], pieces) for side in (0, 1))
        )
    return jax.tree.map(lambda part: part[0], pieces)


def combined_all(value, axis, combine):
    pieces = all_in_one(value, axis)
    return combined_pairwise(pieces, combine)


def rotate(vectors, positions):
    half_width = vectors.shape[-1] // 2
    inv_freq = jnp.power(ROTARY_BASE, -jnp.arange(half_width, dtype=jnp.float32) / half_width)
    angles = positions.astype(jnp.float32)[:, None] * inv_freq[None, :]
    bcast_shape = (angles.shape[0],) + (1,) * (vectors.ndim - 2) + (half_width,)
    cosine = jnp.cos(angles).reshape(bcast_shape)
    sine_part = jnp.sin(angles).reshape(bcast_shape)
    first_half = vectors[..., :half_width]
    second_half = vectors[..., half_width:]
    return jnp.concatenate(
        [
            first_half * cosine - second_half * sine_part,
            second_half * cosine + first_half * sine_part,
        ],
        axis=-1,
    )


def channel_mix(stream, gain, w_gate, w_up, w_down):
    stream_f = stream.astype(jnp.float32)
    scaled = (stream_f * gain.astype(jnp.float32)).astype(jnp.bfloat16)
    square = jnp.sum(stream_f * stream_f, axis=1)
    gate_part = jnp.dot(scaled, w_gate, preferred_element_type=jnp.float32)
    up_part = jnp.dot(scaled, w_up, preferred_element_type=jnp.float32)
    square, gate_sum, up_sum = (
        one_axis_at_a_time(square.astype(jnp.bfloat16), KV).astype(jnp.float32),
        one_axis_at_a_time(gate_part.astype(jnp.bfloat16), KV).astype(jnp.float32),
        one_axis_at_a_time(up_part.astype(jnp.bfloat16), KV).astype(jnp.float32),
    )
    row_scale = lax.rsqrt(square / D + EPSILON)[:, None]
    hidden = (jax.nn.silu(row_scale * gate_sum) * (row_scale * up_sum)).astype(jnp.bfloat16)
    partial_value = jnp.dot(hidden, w_down, preferred_element_type=jnp.float32)
    total_sum = taken_together(partial_value, "tp")
    return (stream_f + 0.5 * total_sum).astype(jnp.bfloat16)


def combine_parts(left, right):
    peak_max = jnp.maximum(left[0], right[0])
    left_scale = jnp.exp(left[0] - peak_max)
    right_scale = jnp.exp(right[0] - peak_max)
    return (
        peak_max,
        left[1] * left_scale + right[1] * right_scale,
        left[2] * left_scale[..., None] + right[2] * right_scale[..., None],
    )


def token_mix(
    stream,
    lengths,
    cache_keys,
    cache_values,
    lambdas,
    head_gain,
    attn_gain,
    w_query,
    w_key,
    w_value,
    w_out,
):
    seq_count = stream.shape[0]
    heads_dev = lambdas.shape[0]
    pos_count = cache_keys.shape[1]
    scale_att = DK ** (-0.5)
    stream_f = stream.astype(jnp.float32)
    scaled = (stream_f * attn_gain.astype(jnp.float32)).astype(jnp.bfloat16)
    square = jnp.sum(stream_f * stream_f, axis=1)
    query_part = jnp.dot(scaled, w_query, preferred_element_type=jnp.float32)
    key_part = jnp.dot(scaled, w_key, preferred_element_type=jnp.float32)
    value_part = jnp.dot(scaled, w_value, preferred_element_type=jnp.float32)
    square, query_sum, key_sum, value_sum = together((square, query_part, key_part, value_part), KV)
    row_scale = lax.rsqrt(square / D + EPSILON)[:, None]
    query = rotate((row_scale * query_sum).reshape(seq_count, heads_dev, 2, DK), lengths).astype(
        jnp.bfloat16
    )
    key_new = rotate((row_scale * key_sum).reshape(seq_count, heads_dev, 2, DK), lengths).astype(
        jnp.bfloat16
    )
    value_new = (row_scale * value_sum).astype(jnp.bfloat16).reshape(seq_count, heads_dev, DV)
    key_rows = cache_keys.reshape(seq_count, pos_count, heads_dev, 2, DK)
    scores = (
        jnp.einsum("bhcd,bphcd->bhcp", query, key_rows, preferred_element_type=jnp.float32)
        * scale_att
    )
    places = lax.axis_index(KV) * pos_count + jnp.arange(pos_count, dtype=jnp.int32)
    live_mask = (places[None, :] < lengths[:, None])[:, None, None, :]
    scores = jnp.where(live_mask, scores, MASKED_SCORE)
    block_max = jnp.max(scores, axis=3)
    weights = jnp.where(live_mask, jnp.exp(scores - block_max[..., None]), 0.0)
    total_sum = jnp.sum(weights, axis=3)
    values = jnp.einsum(
        "bhcp,bphd->bhcd",
        weights.astype(jnp.bfloat16),
        cache_values,
        preferred_element_type=jnp.float32,
    )
    block_max, total_sum, values = combined_all((block_max, total_sum, values), KV, combine_parts)
    own_score = jnp.sum(query.astype(jnp.float32) * key_new.astype(jnp.float32), axis=3) * scale_att
    peak_max = jnp.maximum(block_max, own_score)
    old_scale = jnp.exp(block_max - peak_max)
    fresh_weight = jnp.exp(own_score - peak_max)
    denominator = total_sum * old_scale + fresh_weight
    mixed = (
        values * old_scale[..., None]
        + fresh_weight[..., None] * value_new.astype(jnp.float32)[:, :, None, :]
    ) / denominator[..., None]
    heads_out = mixed[:, :, 0] - lambdas[None, :, None] * mixed[:, :, 1]
    norm_scale = lax.rsqrt(jnp.mean(heads_out * heads_out, axis=2, keepdims=True) + EPSILON)
    normed = (heads_out * norm_scale * head_gain.astype(jnp.float32) * OUTPUT_KEEP).astype(
        jnp.bfloat16
    )
    normed = normed.reshape(seq_count, heads_dev * DV)
    partial_value = jnp.dot(normed, w_out, preferred_element_type=jnp.float32)
    projected = taken_together(partial_value, "tp")
    return (stream_f + projected).astype(jnp.bfloat16)


def local(
    tokens,
    lengths,
    cache_keys,
    cache_values,
    lambdas,
    head_gain,
    attn_gain,
    w_query,
    w_key,
    w_value,
    w_out,
    first_gain,
    first_gate,
    first_up,
    first_down,
    second_gain,
    second_gate,
    second_up,
    second_down,
):
    first = channel_mix(tokens, first_gain, first_gate, first_up, first_down)
    second = token_mix(
        first,
        lengths,
        cache_keys,
        cache_values,
        lambdas,
        head_gain,
        attn_gain,
        w_query,
        w_key,
        w_value,
        w_out,
    )
    return channel_mix(second, second_gain, second_gate, second_up, second_down)


def solution(mesh):
    finer = Mesh(mesh.devices.reshape(4, 4, mesh.shape["tp"]), ("kv_0", "kv_1", "tp"))
    placed = (
        P(None, KV),
        P(),
        P(None, KV, "tp", None),
        P(None, KV, "tp", None),
        P("tp"),
        P(),
        P(KV),
        P(KV, "tp"),
        P(KV, "tp"),
        P(KV, "tp"),
        P("tp", KV),
        P(KV),
        P(KV, "tp"),
        P(KV, "tp"),
        P("tp", KV),
        P(KV),
        P(KV, "tp"),
        P(KV, "tp"),
        P("tp", KV),
    )
    return jax.shard_map(local, mesh=finer, in_specs=placed, out_specs=P(None, KV), check_vma=False)
```

profile of v0, /device:TPU:1, one launch (start us, length us, event | category | flops | bytes accessed | tf_op | source)
XLA Modules:
  0.0 159.8 jit_solution(13834522960345422851)
XLA Ops:
  0.0 0.7 convert_element_type.160
  0.7 0.8 fusion.16
  1.5 0.8 convolution_convert_fusion.2
  2.3 1.1 convolution_convert_fusion.3
  3.4 14.4 %all-reduce.5 = (bf16[16,352]{1,0:T(8,128)(2,1)S(1)}, bf16[16,352]{1,0:T(8,128)(2,1)S(1)}, bf16[16]{0:T(256)(128)(2,1)S(1)}) all-reduce(bf16[16,352]{1,0:T(8,128)(2,1)S(1)} %convolution_convert_fusion.2, bf16[16,352]{1,0:T(8,128)(2,1)S(1)} %convolution_convert_fusion.3, ...), channel_id=1, replica_groups=mesh['kv_0'=4,'kv_1'=4,'tp'=16] {'kv_0'}, use_global_device_ids=true, to_apply=%region_5.0 | all-reduce | flops 11280 | bytes 45120 | tf_op jit(solution)/shard_map/psum | solution.py:21
  17.8 13.3 %all-reduce.3 = (bf16[16,352]{1,0:T(8,128)(2,1)S(1)}, bf16[16,352]{1,0:T(8,128)(2,1)S(1)}, bf16[16]{0:T(256)(128)(2,1)S(1)}) all-reduce(bf16[16,352]{1,0:T(8,128)(2,1)S(1)} %get-tuple-element.14, bf16[16,352]{1,0:T(8,128)(2,1)S(1)} %get-tuple-element.15, ...), channel_id=1, replica_groups=mesh['kv_0'=4,'kv_1'=4,'tp'=16] {'kv_1'}, use_global_device_ids=true, to_apply=%region_6.0 | all-reduce | flops 11280 | bytes 45120 | tf_op jit(solution)/shard_map/psum | solution.py:21
  31.1 1.1 fusion.10
  32.2 0.7 broadcast_in_dim.28
  32.8 16.7 %all-to-all-start = ((f32[16,16,128]{2,1,0:T(8,128)}), f32[16,16,128]{2,1,0:T(8,128)S(1)}, u32[]{:S(2)}, u32[]{:S(2)}) async-start(f32[16,16,128]{2,1,0:T(8,128)} %broadcast_in_dim.28), calls=%async_computation | async-start | bytes 262144 | tf_op jit(solution)/shard_map/all_to_all | solution.py:27
  49.5 0.7 convert_element_type.169
  50.2 0.7 convert_element_type.171
  50.8 7.6 %all-to-all-done = f32[16,16,128]{2,1,0:T(8,128)S(1)} async-done(((f32[16,16,128]{2,1,0:T(8,128)}), f32[16,16,128]{2,1,0:T(8,128)S(1)}, u32[]{:S(2)}, u32[]{:S(2)}) %all-to-all-start) | async-done | bytes 131104 | tf_op jit(solution)/shard_map/all_to_all | solution.py:27
  58.4 0.8 fusion.19
  59.2 0.9 convolution_bitcast_fusion
  60.1 0.9 convolution_bitcast_fusion.2
  61.0 0.9 convolution_bitcast_fusion.1
  62.0 1.0 broadcast_in_dim.30
  62.9 3.6 %all-to-all-start.1 = ((f32[16,1,6160]{2,1,0:T(1,128)}), f32[16,1,6160]{2,1,0:T(1,128)S(1)}, u32[]{:S(2)}, u32[]{:S(2)}) async-start(f32[16,1,6160]{2,1,0:T(1,128)} %broadcast_in_dim.30), calls=%async_computation.1 | async-start | bytes 802816 | tf_op jit(solution)/shard_map/all_to_all | solution.py:27
  66.6 6.4 %copy.202 = bf16[16,1024,1,128]{1,3,0,2:T(8,128)(2,1)} copy(bf16[16,1024,1,128]{3,1,2,0:T(8,128)(2,1)} %param.21) | data formatting | bytes 8388608 | tf_op args[2]
  73.1 3.3 %all-to-all-done.1 = f32[16,1,6160]{2,1,0:T(1,128)S(1)} async-done(((f32[16,1,6160]{2,1,0:T(1,128)}), f32[16,1,6160]{2,1,0:T(1,128)S(1)}, u32[]{:S(2)}, u32[]{:S(2)}) %all-to-all-start.1) | async-done | bytes 394272 | tf_op jit(solution)/shard_map/all_to_all | solution.py:27
  76.4 0.3 reduce_sum.93
  77.2 2.9 %fusion.8 = f32[16,2,1,1024]{3,2,1,0:T(1,128)S(1)} fusion(bf16[16,1024,2,64]{1,3,2,0:T(8,128)(2,1)} %bitcast.96, bf16[16,2,64,1]{2,0,1,3:T(8,128)(2,1)S(1)} %maximum_bitcast_fusion), kind=kOutput, calls=%fused_computation.27 | convolution fusion | flops 4194304 | bytes 4329472 | tf_op jit(solution)/shard_map/bhcd,bphcd->bhcp/dot_general | solution.py:155
  80.0 0.2 fusion.4
  80.3 0.3 fusion.59
  80.7 3.0 %fusion = f32[16,2,128]{2,1,0:T(2,128)S(1)} fusion(bf16[16,1024,1,128]{3,1,2,0:T(8,128)(2,1)} %param.22, pred[16,1024]{1,0:T(8,128)(4,1)S(1)} %broadcast_compare_fusion, f32[16,2]{1,0:T(8,128)S(1)} %fusion.4, f32[16,2,1,1024]{3,2,1,0:T(1,128)S(1)} %fusion.8), kind=kOutput, calls=%fused_computation | convolution fusion | flops 8552448 | bytes 4358272 | tf_op jit(solution)/shard_map/bhcp,bphd->bhcd/dot_general | solution.py:164
  83.8 0.7 broadcast_in_dim.33
  84.5 3.5 %all-to-all-start.2 = ((f32[16,34,128]{2,1,0:T(8,128)}), f32[16,34,128]{2,1,0:T(8,128)S(1)}, u32[]{:S(2)}, u32[]{:S(2)}) async-start(f32[16,34,128]{2,1,0:T(8,128)} %broadcast_in_dim.33), calls=%async_computation.2 | async-start | bytes 655360 | tf_op jit(solution)/shard_map/all_to_all | solution.py:27
  88.7 0.2 multiply_reduce_fusion
  89.0 7.3 %all-to-all-done.2 = f32[16,34,128]{2,1,0:T(8,128)S(1)} async-done(((f32[16,34,128]{2,1,0:T(8,128)}), f32[16,34,128]{2,1,0:T(8,128)S(1)}, u32[]{:S(2)}, u32[]{:S(2)}) %all-to-all-start.2) | async-done | bytes 278560 | tf_op jit(solution)/shard_map/all_to_all | solution.py:27
  97.6 0.2 copy.231
  97.8 0.3 slice.133
  98.1 0.3 slice.128
  98.5 0.1 multiply_add_fusion
  98.7 0.4 slice.137
  99.0 0.4 slice.134
  99.8 0.3 slice.141
  100.1 0.3 slice.138
  100.9 0.1 multiply_add_fusion.2
  101.4 0.2 fusion.31
  101.6 0.7 broadcast_in_dim.34
  102.2 5.4 %all-to-all-start.3 = ((f32[16,16,128]{2,1,0:T(8,128)}), f32[16,16,128]{2,1,0:T(8,128)S(1)}, u32[]{:S(2)}, u32[]{:S(2)}) async-start(f32[16,16,128]{2,1,0:T(8,128)} %broadcast_in_dim.34), calls=%async_computation.3 | async-start | bytes 262144 | tf_op jit(solution)/shard_map/all_to_all | solution.py:27
  107.6 9.2 %all-to-all-done.3 = f32[16,16,128]{2,1,0:T(8,128)S(1)} async-done(((f32[16,16,128]{2,1,0:T(8,128)}), f32[16,16,128]{2,1,0:T(8,128)S(1)}, u32[]{:S(2)}, u32[]{:S(2)}) %all-to-all-start.3) | async-done | bytes 131104 | tf_op jit(solution)/shard_map/all_to_all | solution.py:27
  117.1 0.1 convolution_convert_fusion
  117.2 11.4 %all-reduce.4 = (bf16[16,352]{1,0:T(8,128)(2,1)S(1)}, bf16[16,352]{1,0:T(8,128)(2,1)S(1)}, bf16[16]{0:T(256)(128)(2,1)S(1)}) all-reduce(bf16[16,352]{1,0:T(8,128)(2,1)S(1)} %convolution_convert_fusion, bf16[16,352]{1,0:T(8,128)(2,1)S(1)} %convolution_convert_fusion.1, ...), channel_id=1, replica_groups=mesh['kv_0'=4,'kv_1'=4,'tp'=16] {'kv_0'}, use_global_device_ids=true, to_apply=%region_20.21 | all-reduce | flops 11280 | bytes 45120 | tf_op jit(solution)/shard_map/psum | solution.py:21
  128.6 11.9 %all-reduce.2 = (bf16[16,352]{1,0:T(8,128)(2,1)S(1)}, bf16[16,352]{1,0:T(8,128)(2,1)S(1)}, bf16[16]{0:T(256)(128)(2,1)S(1)}) all-reduce(bf16[16,352]{1,0:T(8,128)(2,1)S(1)} %get-tuple-element.11, bf16[16,352]{1,0:T(8,128)(2,1)S(1)} %get-tuple-element.12, ...), channel_id=1, replica_groups=mesh['kv_0'=4,'kv_1'=4,'tp'=16] {'kv_1'}, use_global_device_ids=true, to_apply=%region_21.22 | all-reduce | flops 11280 | bytes 45120 | tf_op jit(solution)/shard_map/psum | solution.py:21
  140.5 0.2 fusion.11
  140.7 18.5 %all_to_all.26 = f32[16,16,128]{2,1,0:T(8,128)S(1)} all-to-all(f32[16,16,128]{2,1,0:T(8,128)S(1)} %broadcast_in_dim.35), channel_id=1, replica_groups=mesh['kv_0'=4,'kv_1'=4,'tp'=16] {'tp'}, dimensions={0} | all-to-all | bytes 262144 | tf_op jit(solution)/shard_map/all_to_all | solution.py:27
  159.2 0.6 fusion.24
  (86 shorter events, 3.9 us)
Async XLA Ops:
  0.0 1.5 copy-start
  32.8 25.6 %all-to-all-start = ((f32[16,16,128]{2,1,0:T(8,128)}), f32[16,16,128]{2,1,0:T(8,128)S(1)}, u32[]{:S(2)}, u32[]{:S(2)}) async-start(f32[16,16,128]{2,1,0:T(8,128)} %broadcast_in_dim.28), calls=%async_computation | async-start | bytes 262144 | tf_op jit(solution)/shard_map/all_to_all | solution.py:27
  62.9 13.5 %all-to-all-start.1 = ((f32[16,1,6160]{2,1,0:T(1,128)}), f32[16,1,6160]{2,1,0:T(1,128)S(1)}, u32[]{:S(2)}, u32[]{:S(2)}) async-start(f32[16,1,6160]{2,1,0:T(1,128)} %broadcast_in_dim.30), calls=%async_computation.1 | async-start | bytes 802816 | tf_op jit(solution)/shard_map/all_to_all | solution.py:27
  66.6 6.4 %copy-start.3 = (s32[16]{0:T(128)S(1)}, s32[16]{0:T(128)}, u32[]{:S(2)}) copy-start(s32[16]{0:T(128)} %param.20) | copy-start | bytes 196
  77.2 11.5 %copy-start.6 = (bf16[128]{0:T(256)(128)(2,1)S(1)}, bf16[128]{0:T(256)(128)(2,1)}, u32[]{:S(2)}) copy-start(bf16[128]{0:T(256)(128)(2,1)} %param.24) | copy-start | bytes 772
  80.6 20.7 %copy-start.5 = (bf16[128,128]{1,0:T(8,128)(2,1)S(1)}, bf16[128,128]{1,0:T(8,128)(2,1)}, u32[]{:S(2)}) copy-start(bf16[128,128]{1,0:T(8,128)(2,1)} %param.29) | copy-start | bytes 98308
  80.6 26.9 %copy-start.7 = (bf16[128]{0:T(256)(128)(2,1)S(1)}, bf16[128]{0:T(256)(128)(2,1)}, u32[]{:S(2)}) copy-start(bf16[128]{0:T(256)(128)(2,1)} %param.34) | copy-start | bytes 772
  80.7 36.3 %copy-start.1 = (bf16[128,352]{0,1:T(8,128)(2,1)S(1)}, bf16[128,352]{0,1:T(8,128)(2,1)}, u32[]{:S(2)}) copy-start(bf16[128,352]{0,1:T(8,128)(2,1)} %param.35) | copy-start | bytes 270340
  80.7 36.4 %copy-start.2 = (bf16[128,352]{0,1:T(8,128)(2,1)S(1)}, bf16[128,352]{0,1:T(8,128)(2,1)}, u32[]{:S(2)}) copy-start(bf16[128,352]{0,1:T(8,128)(2,1)} %param.36) | copy-start | bytes 270340
  80.7 59.8 %copy-start.4 = (bf16[352,128]{1,0:T(8,128)(2,1)S(1)}, bf16[352,128]{1,0:T(8,128)(2,1)}, u32[]{:S(2)}) copy-start(bf16[352,128]{1,0:T(8,128)(2,1)} %param.37) | copy-start | bytes 270340
  84.5 11.8 %all-to-all-start.2 = ((f32[16,34,128]{2,1,0:T(8,128)}), f32[16,34,128]{2,1,0:T(8,128)S(1)}, u32[]{:S(2)}, u32[]{:S(2)}) async-start(f32[16,34,128]{2,1,0:T(8,128)} %broadcast_in_dim.33), calls=%async_computation.2 | async-start | bytes 655360 | tf_op jit(solution)/shard_map/all_to_all | solution.py:27
  102.2 14.6 %all-to-all-start.3 = ((f32[16,16,128]{2,1,0:T(8,128)}), f32[16,16,128]{2,1,0:T(8,128)S(1)}, u32[]{:S(2)}, u32[]{:S(2)}) async-start(f32[16,16,128]{2,1,0:T(8,128)} %broadcast_in_dim.34), calls=%async_computation.3 | async-start | bytes 262144 | tf_op jit(solution)/shard_map/all_to_all | solution.py:27
where the time goes:
time: 161 us; the launch traced here: 160 us
  blocking collectives  69.4 us (43%)
  starting transfers between devices  29.1 us (18%)
  waiting for transfers between devices  27.3 us (17%)
  local copies, waits for them, and re-layouts  14 us (9%)
  matrix products  12.1 us (8%)
  other arithmetic  6.69 us (4%)
    psum x4, blocking collectives, one_axis_at_a_time(): value = lax.psum(value, axis)  51 us
    all_to_all x4, starting transfers between devices, copy_for_each(): return lax.all_to_all(copies, axis, split_axis=0, concat_axis=0, tiled=True)  29.1 us
    all_to_all x4, waiting for transfers between devices, copy_for_each(): return lax.all_to_all(copies, axis, split_axis=0, concat_axis=0, tiled=True)  27.3 us
    all_to_all x1, blocking collectives, copy_for_each(): return lax.all_to_all(copies, axis, split_axis=0, concat_axis=0, tiled=True)  18.5 us
    unnamed x24, local copies, waits for them, and re-layouts  7.09 us
  transfers between devices with their start and end apart: 4, of which 4 were waited for; matrix products, arithmetic and copies ran while one was open for 5% of the time, Pallas kernels for 0%

commit v1 on v0

v1 whole, which is shorter than its diff:
```python
import functools

import jax
import jax.numpy as jnp
import numpy as np
from jax import lax
from jax.experimental import pallas as pl
from jax.experimental.pallas import tpu as pltpu
from jax.sharding import PartitionSpec as P

MESH = pl.DeviceIdType.MESH
F32 = jnp.float32
BF16 = jnp.bfloat16

D = 2048
DK = 64
DV = 128
SIDE = 4
DEEP = 8
GROUP = 16
SEQS = 16
BLOCK = 1024
UNITS = 352
WIDE = 384

EPSILON = 1e-06
ROTARY_BASE = 10000.0
OUTPUT_KEEP = 0.8
MASKED_SCORE = -1e30
NT = (((1,), (1,)), ((), ()))


def lane_of(shape):
    return lax.broadcasted_iota(jnp.int32, shape, len(shape) - 1)


def row_of(shape):
    return lax.broadcasted_iota(jnp.int32, shape, len(shape) - 2)


def rounded(value):
    return value.astype(BF16).astype(F32)


def added(buf):
    total = buf[0].astype(F32)
    for i in range(1, GROUP):
        total = total + buf[i].astype(F32)
    return total


def kernel(
    lengths,
    lambdas,
    inv_freq,
    tokens,
    keys,
    values,
    head_gain,
    attn_gain,
    w_query,
    w_key,
    w_value,
    w_out,
    first_gain,
    first_gate,
    first_up,
    first_down,
    second_gain,
    second_gate,
    second_up,
    second_down,
    out,
    v_tokens,
    v_freq,
    v_gains,
    v_wide,
    v_down,
    v_qkv,
    v_out,
    v_keys,
    v_values,
    b_mix1,
    b_down1,
    b_qkv,
    b_attn,
    b_proj,
    b_mix2,
    b_down2,
    local_sem,
    send_sem,
    recv_sem,
):
    kv, tp = lax.axis_index("kv"), lax.axis_index("tp")
    y, x = kv // SIDE, kv % SIDE
    z, core = tp // 2, tp % 2

    started = []

    def fetch(src, dst):
        copy = pltpu.make_async_copy(src, dst, local_sem.at[len(started)])
        copy.start()
        started.append(copy)
        return copy

    c_tokens = fetch(tokens, v_tokens)
    c_gain1 = fetch(first_gain, v_gains.at[0])
    c_gate1 = fetch(first_gate, v_wide.at[0, pl.ds(0, UNITS)])
    c_up1 = fetch(first_up, v_wide.at[0, pl.ds(WIDE, UNITS)])
    c_down1 = fetch(first_down, v_down.at[0, pl.ds(0, UNITS)])
    c_freq = fetch(inv_freq, v_freq)
    c_gain2 = fetch(attn_gain, v_gains.at[1])
    c_q = fetch(w_query, v_qkv.at[:, pl.ds(0, 128)])
    c_k = fetch(w_key, v_qkv.at[:, pl.ds(128, 128)])
    c_v = fetch(w_value, v_qkv.at[:, pl.ds(256, 128)])
    c_keys = fetch(keys, v_keys)
    c_values = fetch(values, v_values)
    c_gain3 = fetch(head_gain, v_gains.at[2])
    c_out = fetch(w_out, v_out)
    c_gain4 = fetch(second_gain, v_gains.at[3])
    c_gate2 = fetch(second_gate, v_wide.at[1, pl.ds(0, UNITS)])
    c_up2 = fetch(second_up, v_wide.at[1, pl.ds(WIDE, UNITS)])
    c_down2 = fetch(second_down, v_down.at[1, pl.ds(0, UNITS)])

    reach = lambda step, side: min(step, side - step)
    plane = sorted(
        ((dy, dx) for dy in range(SIDE) for dx in range(SIDE) if dy or dx),
        key=lambda s: -reach(s[0], SIDE) - reach(s[1], SIDE),
    )
    column = sorted(
        ((dz, dc) for dz in range(DEEP) for dc in range(2) if dz or dc),
        key=lambda s: -2 * reach(s[0], DEEP) - s[1],
    )
    kv_peers = [(((y + dy) % SIDE) * SIDE + (x + dx) % SIDE, tp) for dy, dx in plane]
    tp_peers = [(kv, ((z + dz) % DEEP) * 2 + (core + dc) % 2) for dz, dc in column]

    barrier = pltpu.get_barrier_semaphore()
    for peer in kv_peers + tp_peers:
        pl.semaphore_signal(barrier, inc=1, device_id=peer, device_id_type=MESH)

    def send(phase, buf, me, peers):
        for peer in peers:
            pltpu.make_async_remote_copy(
                src_ref=buf.at[me],
                dst_ref=buf.at[me],
                send_sem=send_sem.at[phase],
                recv_sem=recv_sem.at[phase],
                device_id=peer,
                device_id_type=MESH,
            ).start()

    def settle(buf, sem):
        others = buf.at[pl.ds(0, GROUP - 1)]
        pltpu.make_async_copy(others, others, sem).wait()

    for half in range(2):
        for at in (UNITS, WIDE + UNITS):
            v_wide[half, pl.ds(at, WIDE - UNITS)] = jnp.zeros((WIDE - UNITS, 128), BF16)
        v_down[half, pl.ds(UNITS, WIDE - UNITS)] = jnp.zeros((WIDE - UNITS, 128), BF16)

    def gain_row(at):
        return v_gains[at].astype(F32)

    wide_lane = lane_of((SEQS, 2 * WIDE))
    tile_lane = lane_of((SEQS, 128))
    SQ = UNITS - 256

    def mix_partial(stream, gain, at, buf):
        scaled = (stream * gain).astype(BF16)
        part = lax.dot_general(scaled, v_wide[at], NT, preferred_element_type=F32)
        square = jnp.sum(stream * stream, axis=1, keepdims=True)
        high = rounded(square)
        part = jnp.where(wide_lane == UNITS, high, part)
        part = jnp.where(wide_lane == UNITS + 1, square - high, part)
        buf[kv] = part.astype(BF16)

    def mix_hidden(buf):
        total = added(buf)
        third = total[:, 256:384]
        own = (tile_lane == SQ) | (tile_lane == SQ + 1)
        square = jnp.sum(jnp.where(own, third, 0.0), axis=1, keepdims=True)
        scale = lax.rsqrt(square / D + EPSILON)
        gate, up = scale * total[:, :WIDE], scale * total[:, WIDE:]
        return (jax.nn.silu(gate) * up).astype(BF16)

    c_tokens.wait()
    c_gain1.wait()
    c_gate1.wait()
    c_up1.wait()
    stream = v_tokens[...].astype(F32)
    mix_partial(stream, gain_row(0), 0, b_mix1)
    pl.semaphore_wait(barrier, 2 * (GROUP - 1))
    send(0, b_mix1, kv, kv_peers)

    c_freq.wait()
    small = (SEQS, 128)
    row = row_of(small)
    lens = jnp.zeros(small, jnp.int32)
    for b in range(SEQS):
        lens = jnp.where(row == b, lengths[b], lens)
    angles = lens.astype(F32) * v_freq[...]
    cosine, sine = jnp.cos(angles), jnp.sin(angles)
    in_half = tile_lane % DK < DK // 2
    sine = jnp.where(in_half, -sine, sine)
    c_down1.wait()
    for copy in (c_gain2, c_q, c_k, c_v):
        copy.wait()

    settle(b_mix1, recv_sem.at[0])
    hidden = mix_hidden(b_mix1)
    b_down1[tp] = jnp.dot(hidden, v_down[0], preferred_element_type=F32).astype(BF16)
    send(1, b_down1, tp, tp_peers)
    for copy in (c_keys, c_values, c_gain3, c_out, c_gain4, c_gate2, c_up2, c_down2):
        copy.wait()
    settle(b_down1, recv_sem.at[1])
    first = rounded(stream + 0.5 * added(b_down1))

    scaled = (first * gain_row(1)).astype(BF16)
    part = jnp.dot(scaled, v_qkv[...], preferred_element_type=F32)
    square = jnp.sum(first * first, axis=1, keepdims=True)
    lane8 = lane_of((8, 128))
    high = rounded(square)
    low = square - high
    stats = jnp.zeros((8, 128), F32)
    for at, column_of in enumerate((high[:8], high[8:], low[:8], low[8:])):
        stats = jnp.where(lane8 == at, column_of, stats)
    for at in range(3):
        b_qkv[kv, pl.ds(at * SEQS, SEQS)] = part[:, at * 128 : (at + 1) * 128].astype(BF16)
    b_qkv[kv, pl.ds(3 * SEQS, 8)] = stats.astype(BF16)
    send(2, b_qkv, kv, kv_peers)
    settle(b_qkv, recv_sem.at[2])
    total = added(b_qkv)
    stats = total[3 * SEQS :]
    squares = [
        jnp.sum(jnp.where((lane8 == at) | (lane8 == at + 2), stats, 0.0), axis=1, keepdims=True)
        for at in range(2)
    ]
    scale = lax.rsqrt(jnp.concatenate(squares, axis=0) / D + EPSILON)

    def rotate(vectors):
        swapped = jnp.where(in_half, pltpu.roll(vectors, 96, 1), pltpu.roll(vectors, 32, 1))
        return rounded(vectors * cosine + swapped * sine)

    query = rotate(scale * total[:SEQS])
    key_new = rotate(scale * total[SEQS : 2 * SEQS])
    value_new = rounded(scale * total[2 * SEQS : 3 * SEQS])

    scale_att = DK ** (-0.5)
    front = tile_lane < DK
    both = jnp.concatenate([jnp.where(front, query, 0.0), jnp.where(front, 0.0, query)], axis=0)
    row2 = row_of((2 * SEQS, 128)) % SEQS
    scores = jnp.zeros((2 * SEQS, BLOCK), F32)
    for pair in range(SEQS // 2):
        b = 2 * pair
        lhs = jnp.concatenate(
            [jnp.where(row2 == b + k, both, 0.0).astype(BF16) for k in range(2)], axis=1
        )
        rhs = jnp.concatenate([v_keys[b + k] for k in range(2)], axis=1)
        scores = scores + lax.dot_general(lhs, rhs, NT, preferred_element_type=F32)
    lens2 = jnp.concatenate([lens, lens], axis=0)
    lens_wide = jnp.concatenate([lens2] * (BLOCK // 128), axis=1)
    live = kv * BLOCK + lane_of((2 * SEQS, BLOCK)) < lens_wide
    scores = jnp.where(live, scores * scale_att, MASKED_SCORE)
    block_max = jnp.max(scores, axis=1, keepdims=True)
    weights = jnp.where(live, jnp.exp(scores - block_max), 0.0)
    block_sum = jnp.sum(weights, axis=1, keepdims=True)
    weights = weights.astype(BF16)
    mixed = jnp.zeros((2 * SEQS, DV), F32)
    for pair in range(SEQS // 2):
        b = 2 * pair
        rhs = jnp.concatenate([v_values[b + k] for k in range(2)], axis=1)
        product = jnp.dot(weights, rhs, preferred_element_type=F32)
        for k in range(2):
            mixed = jnp.where(row2 == b + k, product[:, k * DV : (k + 1) * DV], mixed)
    b_attn[kv, pl.ds(0, 2 * SEQS)] = mixed.astype(BF16)

    def packed(columns):
        tile = jnp.zeros((8, 128), F32)
        for at, column_of in enumerate(columns):
            tile = jnp.where(lane8 == at, column_of, tile)
        return tile

    quarters = [slice(8 * k, 8 * k + 8) for k in range(4)]
    peak = packed([block_max[q] for q in quarters])
    weight = packed([block_sum[q] for q in quarters])
    peak_high = rounded(peak)
    peak_mid = rounded(peak - peak_high)
    weight_high = rounded(weight)
    stats = peak_high + pltpu.roll(peak_mid, 4, 1) + pltpu.roll(peak - peak_high - peak_mid, 8, 1)
    stats = stats + pltpu.roll(weight_high, 12, 1) + pltpu.roll(weight - weight_high, 16, 1)
    b_attn[kv, pl.ds(2 * SEQS, 8)] = stats.astype(BF16)
    send(3, b_attn, kv, kv_peers)

    product = query * key_new * scale_att
    own = [jnp.sum(jnp.where(f, product, 0.0), axis=1, keepdims=True) for f in (front, ~front)]
    own_score = packed([own[k // 2][8 * (k % 2) : 8 * (k % 2) + 8] for k in range(4)])

    settle(b_attn, recv_sem.at[3])
    peaks, sums = [], []
    for i in range(GROUP):
        tile = b_attn[i, pl.ds(2 * SEQS, 8)].astype(F32)
        peaks.append(tile + pltpu.roll(tile, 124, 1) + pltpu.roll(tile, 120, 1))
        sums.append(pltpu.roll(tile, 116, 1) + pltpu.roll(tile, 112, 1))
    peak = functools.reduce(jnp.maximum, peaks, own_score)
    shares = [jnp.exp(p - peak) for p in peaks]
    fresh = jnp.exp(own_score - peak)
    total_sum = fresh
    for share, s in zip(shares, sums):
        total_sum = total_sum + share * s
    inverse = 1.0 / total_sum
    fresh = fresh * inverse
    shares = [share * inverse for share in shares]
    rows = []
    for k in range(4):
        half = 8 * (k % 2)
        acc = fresh[:, k : k + 1] * value_new[half : half + 8]
        for i in range(GROUP):
            acc = acc + shares[i][:, k : k + 1] * b_attn[i, pl.ds(8 * k, 8)].astype(F32)
        rows.append(acc)
    heads = jnp.concatenate(rows[:2], axis=0) - lambdas[0] * jnp.concatenate(rows[2:], axis=0)
    spread = jnp.sum(heads * heads, axis=1, keepdims=True) / DV
    normed = heads * lax.rsqrt(spread + EPSILON) * gain_row(2) * OUTPUT_KEEP
    b_proj[tp] = jnp.dot(normed.astype(BF16), v_out[...], preferred_element_type=F32).astype(BF16)
    send(4, b_proj, tp, tp_peers)
    settle(b_proj, recv_sem.at[4])
    second = rounded(first + added(b_proj))

    mix_partial(second, gain_row(3), 1, b_mix2)
    send(5, b_mix2, kv, kv_peers)
    settle(b_mix2, recv_sem.at[5])
    hidden = mix_hidden(b_mix2)
    b_down2[tp] = jnp.dot(hidden, v_down[1], preferred_element_type=F32).astype(BF16)
    send(6, b_down2, tp, tp_peers)
    settle(b_down2, recv_sem.at[6])
    out[...] = (second + 0.5 * added(b_down2)).astype(BF16)

    for phase, buf in enumerate((b_mix1, b_down1, b_qkv, b_attn, b_proj, b_mix2, b_down2)):
        settle(buf, send_sem.at[phase])


def local(
    tokens,
    lengths,
    cache_keys,
    cache_values,
    lambdas,
    head_gain,
    attn_gain,
    w_query,
    w_key,
    w_value,
    w_out,
    first_gain,
    first_gate,
    first_up,
    first_down,
    second_gain,
    second_gate,
    second_up,
    second_down,
):
    inv_freq = (ROTARY_BASE ** (-(np.arange(128) % 32) / 32.0)).astype(np.float32)
    flat = (SEQS, BLOCK, DV)
    operands = (
        lengths,
        lambdas,
        jnp.asarray(inv_freq).reshape(1, 128),
        tokens,
        cache_keys.reshape(flat),
        cache_values.reshape(flat),
        head_gain.reshape(1, 128),
        attn_gain.reshape(1, 128),
        w_query,
        w_key,
        w_value,
        w_out,
        first_gain.reshape(1, 128),
        first_gate.T,
        first_up.T,
        first_down,
        second_gain.reshape(1, 128),
        second_gate.T,
        second_up.T,
        second_down,
    )
    smem = pl.BlockSpec(memory_space=pltpu.SMEM)
    hbm = pl.BlockSpec(memory_space=pltpu.HBM)
    return pl.pallas_call(
        kernel,
        name="layer",
        out_shape=jax.ShapeDtypeStruct((SEQS, 128), BF16),
        in_specs=[smem, smem] + [hbm] * (len(operands) - 2),
        out_specs=pl.BlockSpec(memory_space=pltpu.VMEM),
        scratch_shapes=[
            pltpu.VMEM((SEQS, 128), BF16),
            pltpu.VMEM((1, 128), F32),
            pltpu.VMEM((4, 1, 128), BF16),
            pltpu.VMEM((2, 2 * WIDE, 128), BF16),
            pltpu.VMEM((2, WIDE, 128), BF16),
            pltpu.VMEM((128, 384), BF16),
            pltpu.VMEM((128, 128), BF16),
            pltpu.VMEM(flat, BF16),
            pltpu.VMEM(flat, BF16),
            pltpu.VMEM((GROUP, SEQS, 2 * WIDE), BF16),
            pltpu.VMEM((GROUP, SEQS, 128), BF16),
            pltpu.VMEM((GROUP, 3 * SEQS + 8, 128), BF16),
            pltpu.VMEM((GROUP, 2 * SEQS + 8, 128), BF16),
            pltpu.VMEM((GROUP, SEQS, 128), BF16),
            pltpu.VMEM((GROUP, SEQS, 2 * WIDE), BF16),
            pltpu.VMEM((GROUP, SEQS, 128), BF16),
            pltpu.SemaphoreType.DMA((18,)),
            pltpu.SemaphoreType.DMA((7,)),
            pltpu.SemaphoreType.DMA((7,)),
        ],
        compiler_params=pltpu.CompilerParams(
            collective_id=0, has_side_effects=True, vmem_limit_bytes=67_043_328
        ),
    )(*operands)


def solution(mesh):
    placed = (
        P(None, "kv"),
        P(),
        P(None, "kv", "tp", None),
        P(None, "kv", "tp", None),
        P("tp"),
        P(),
        P("kv"),
        P("kv", "tp"),
        P("kv", "tp"),
        P("kv", "tp"),
        P("tp", "kv"),
        P("kv"),
        P("kv", "tp"),
        P("kv", "tp"),
        P("tp", "kv"),
        P("kv"),
        P("kv", "tp"),
        P("kv", "tp"),
        P("tp", "kv"),
    )
    return jax.shard_map(
        local, mesh=mesh, in_specs=placed, out_specs=P(None, "kv"), check_vma=False
    )
```

time: 161 us -> 55.7 us (0.35)
  blocking collectives: 69.4 us -> 0 us
  Pallas kernels: 0 us -> 53.7 us
  starting transfers between devices: 29.1 us -> 0 us
  waiting for transfers between devices: 27.3 us -> 0 us
  local copies, waits for them, and re-layouts: 14 us -> 1.28 us
  matrix products: 12.1 us -> 0 us
  other arithmetic: 6.69 us -> 0 us
    pallas_call x0 -> x1, Pallas kernels: none -> 53.7 us  [local(): pl.pallas_call(kernel, name='layer', out_shape=jax.ShapeDtypeStruct((SEQS...]
    psum x4 -> x0, blocking collectives: 51 us -> none  [one_axis_at_a_time(): value = lax.psum(value, axis)]
    all_to_all x4 -> x0, starting transfers between devices: 29.1 us -> none  [copy_for_each(): return lax.all_to_all(copies, axis, split_axis=0, concat_axis=0, tiled=True)]
    all_to_all x4 -> x0, waiting for transfers between devices: 27.3 us -> none  [copy_for_each(): return lax.all_to_all(copies, axis, split_axis=0, concat_axis=0, tiled=True)]
    all_to_all x1 -> x0, blocking collectives: 18.5 us -> none  [copy_for_each(): return lax.all_to_all(copies, axis, split_axis=0, concat_axis=0, tiled=True)]
    dot_general x12 -> x0, matrix products: 12.1 us -> none  [the longest x1 2.98 us: token_mix(): jnp.einsum('bhcp,bphd->bhcd', weights.astype(jnp.bfloat16), cache_values,...]
    unnamed x24 -> x1, local copies, waits for them, and re-layouts: 7.09 us -> 1.28 us
    broadcast_in_dim x5 -> x0, local copies, waits for them, and re-layouts: 3.03 us -> none  [copy_for_each(): copies = jnp.broadcast_to(value, (lax.axis_size(axis), *value.shape))]
  transfers between devices with their start and end apart: 4 -> 0, of which waited for: 4 -> 0; matrix products, arithmetic and copies ran while one was open for 5% -> 0% of each run, Pallas kernels for 0% -> 0%
where the time goes in v1:
time: 55.7 us; the launch traced here: 55.6 us
  Pallas kernels  53.7 us (96%)
  local copies, waits for them, and re-layouts  1.28 us (2%)
  between operations  0.66 us (1%)
    pallas_call x1, Pallas kernels, local(): pl.pallas_call(kernel, name='layer', out_shape=jax.ShapeDtypeStruct((SEQS...  53.7 us
    unnamed x1, local copies, waits for them, and re-layouts  1.28 us

profile of v1, /device:TPU:1, one launch (start us, length us, event | category | flops | bytes accessed | tf_op | source)
XLA Modules:
  0.0 55.6 jit_solution(11381582773786247729)
XLA Ops:
  0.7 53.7 %layer.1 = bf16[16,128]{1,0:T(8,128)(2,1)} custom-call(s32[16]{0:T(128)} %lengths.1, f32[1]{0:T(128)S(6)} %copy.22.lambdas, f32[1,128]{1,0:T(1,128)} %constant.6.inv_freq, bf16[16,128]{1,0:T(8,128)(2,1)} %tokens.1, bf16[16,1024,128]{2,1,0:T(8,128)(2,1)} %bitcast.10, bf16[16,1024,128]{2,1,0:T(8,128)(2,1)} %bitcast.11, bf16[1,128]{1,0:T(2,128)(2,1)} %bitcast.16, ...), custom_call_target="tpu_custom_call" | custom-call | tf_op jit(solution)/shard_map/layer/pallas_call | solution.py:388
  54.3 1.3 %copy.23 = bf16[16,128]{1,0:T(8,128)(2,1)} copy(bf16[16,128]{1,0:T(8,128)(2,1)} %layer.1) | data formatting | bytes 8192

commit v2 on v1

v2 whole, which is shorter than its diff:
```python
import functools

import jax
import jax.numpy as jnp
import numpy as np
from jax import lax
from jax.experimental import pallas as pl
from jax.experimental.pallas import tpu as pltpu
from jax.sharding import PartitionSpec as P

MESH = pl.DeviceIdType.MESH
F32 = jnp.float32
BF16 = jnp.bfloat16

D = 2048
DK = 64
DV = 128
SIDE = 4
DEEP = 8
GROUP = 16
SEQS = 16
BLOCK = 1024
UNITS = 352
WIDE = 384

EPSILON = 1e-06
ROTARY_BASE = 10000.0
OUTPUT_KEEP = 0.8
MASKED_SCORE = -1e30
NT = (((1,), (1,)), ((), ()))


def lane_of(shape):
    return lax.broadcasted_iota(jnp.int32, shape, len(shape) - 1)


def row_of(shape):
    return lax.broadcasted_iota(jnp.int32, shape, len(shape) - 2)


def rounded(value):
    return value.astype(BF16).astype(F32)


def added(buf):
    total = buf[0].astype(F32)
    for i in range(1, GROUP):
        total = total + buf[i].astype(F32)
    return total


def kernel(
    lengths,
    lambdas,
    inv_freq,
    tokens,
    keys,
    values,
    head_gain,
    attn_gain,
    w_query,
    w_key,
    w_value,
    w_out,
    first_gain,
    first_gate,
    first_up,
    first_down,
    second_gain,
    second_gate,
    second_up,
    second_down,
    out,
    v_tokens,
    v_freq,
    v_gains,
    v_wide,
    v_down,
    v_qkv,
    v_out,
    v_keys,
    v_values,
    v_keys_t,
    v_result,
    s_lengths,
    b_mix1,
    b_down1,
    b_query,
    b_fresh,
    b_attn,
    b_proj,
    b_mix2,
    b_down2,
    local_sem,
    send_sem,
    recv_sem,
):
    kv, tp = lax.axis_index("kv"), lax.axis_index("tp")
    y, x = kv // SIDE, kv % SIDE
    z, core = tp // 2, tp % 2

    reach = lambda step, side: min(step, side - step)
    plane = sorted(
        ((dy, dx) for dy in range(SIDE) for dx in range(SIDE) if dy or dx),
        key=lambda s: -reach(s[0], SIDE) - reach(s[1], SIDE),
    )
    column = sorted(
        ((dz, dc) for dz in range(DEEP) for dc in range(2) if dz or dc),
        key=lambda s: -2 * reach(s[0], DEEP) - s[1],
    )
    kv_peers = [(((y + dy) % SIDE) * SIDE + (x + dx) % SIDE, tp) for dy, dx in plane]
    tp_peers = [(kv, ((z + dz) % DEEP) * 2 + (core + dc) % 2) for dz, dc in column]

    barrier = pltpu.get_barrier_semaphore()
    for peer in kv_peers + tp_peers:
        pl.semaphore_signal(barrier, inc=1, device_id=peer, device_id_type=MESH)

    started = []

    def fetch(src, dst):
        copy = pltpu.make_async_copy(src, dst, local_sem.at[len(started)])
        copy.start()
        started.append(copy)
        return copy

    c_tokens = fetch(tokens, v_tokens)
    c_gain1 = fetch(first_gain, v_gains.at[0])
    c_gate1 = fetch(first_gate, v_wide.at[0, pl.ds(0, UNITS)])
    c_up1 = fetch(first_up, v_wide.at[0, pl.ds(WIDE, UNITS)])
    c_lengths = fetch(lengths, s_lengths)
    c_keys = fetch(keys, v_keys)
    c_down1 = fetch(first_down, v_down.at[0, pl.ds(0, UNITS)])
    c_freq = fetch(inv_freq, v_freq)
    c_gain2 = fetch(attn_gain, v_gains.at[1])
    c_q = fetch(w_query, v_qkv.at[:, pl.ds(0, 128)])
    c_k = fetch(w_key, v_qkv.at[:, pl.ds(128, 128)])
    c_v = fetch(w_value, v_qkv.at[:, pl.ds(256, 128)])
    c_values = fetch(values, v_values)
    c_gain3 = fetch(head_gain, v_gains.at[2])
    c_out = fetch(w_out, v_out)
    c_gain4 = fetch(second_gain, v_gains.at[3])
    c_gate2 = fetch(second_gate, v_wide.at[1, pl.ds(0, UNITS)])
    c_up2 = fetch(second_up, v_wide.at[1, pl.ds(WIDE, UNITS)])
    c_down2 = fetch(second_down, v_down.at[1, pl.ds(0, UNITS)])

    def send(phase, buf, me, peers):
        for peer in peers:
            pltpu.make_async_remote_copy(
                src_ref=buf.at[me],
                dst_ref=buf.at[me],
                send_sem=send_sem.at[phase],
                recv_sem=recv_sem.at[phase],
                device_id=peer,
                device_id_type=MESH,
            ).start()

    def settle(buf, sem):
        others = buf.at[pl.ds(0, GROUP - 1)]
        pltpu.make_async_copy(others, others, sem).wait()

    for half in range(2):
        for at in (UNITS, WIDE + UNITS):
            v_wide[half, pl.ds(at, WIDE - UNITS)] = jnp.zeros((WIDE - UNITS, 128), BF16)
        v_down[half, pl.ds(UNITS, WIDE - UNITS)] = jnp.zeros((WIDE - UNITS, 128), BF16)

    def gain_row(at):
        return v_gains[at].astype(F32)

    wide_lane = lane_of((SEQS, 2 * WIDE))
    tile_lane = lane_of((SEQS, 128))
    SQ = UNITS - 256

    def mix_partial(stream, gain, at, buf):
        scaled = (stream * gain).astype(BF16)
        part = lax.dot_general(scaled, v_wide[at], NT, preferred_element_type=F32)
        square = jnp.sum(stream * stream, axis=1, keepdims=True)
        high = rounded(square)
        part = jnp.where(wide_lane == UNITS, high, part)
        part = jnp.where(wide_lane == UNITS + 1, square - high, part)
        buf[kv] = part.astype(BF16)

    def mix_hidden(buf):
        total = added(buf)
        third = total[:, 256:384]
        own = (tile_lane == SQ) | (tile_lane == SQ + 1)
        square = jnp.sum(jnp.where(own, third, 0.0), axis=1, keepdims=True)
        scale = lax.rsqrt(square / D + EPSILON)
        gate, up = scale * total[:, :WIDE], scale * total[:, WIDE:]
        return (jax.nn.silu(gate) * up).astype(BF16)

    c_tokens.wait()
    c_gain1.wait()
    c_gate1.wait()
    c_up1.wait()
    stream = v_tokens[...].astype(F32)
    mix_partial(stream, gain_row(0), 0, b_mix1)
    pl.semaphore_wait(barrier, 2 * (GROUP - 1))
    send(0, b_mix1, kv, kv_peers)

    c_freq.wait()
    c_lengths.wait()
    small = (SEQS, 128)
    row = row_of(small)
    lens = jnp.zeros(small, jnp.int32)
    for b in range(SEQS):
        lens = jnp.where(row == b, s_lengths[b], lens)
    angles = lens.astype(F32) * v_freq[...]
    cosine, sine = jnp.cos(angles), jnp.sin(angles)
    in_half = tile_lane % DK < DK // 2
    sine = jnp.where(in_half, -sine, sine)
    c_keys.wait()

    def turn(b, carry):
        v_keys_t[pl.ds(pl.multiple_of(b * 128, 128), 128)] = v_keys[b].T
        return carry

    lax.fori_loop(0, SEQS, turn, 0)
    c_down1.wait()
    for copy in (c_gain2, c_q, c_k, c_v):
        copy.wait()

    settle(b_mix1, recv_sem.at[0])
    hidden = mix_hidden(b_mix1)
    b_down1[tp] = jnp.dot(hidden, v_down[0], preferred_element_type=F32).astype(BF16)
    send(1, b_down1, tp, tp_peers)
    for copy in (c_values, c_gain3, c_out, c_gain4, c_gate2, c_up2, c_down2):
        copy.wait()
    settle(b_down1, recv_sem.at[1])
    first = rounded(stream + 0.5 * added(b_down1))

    scaled = (first * gain_row(1)).astype(BF16)
    part = jnp.dot(scaled, v_qkv[...], preferred_element_type=F32)
    square = jnp.sum(first * first, axis=1, keepdims=True)
    lane8 = lane_of((8, 128))
    high = rounded(square)
    low = square - high
    stats = jnp.zeros((8, 128), F32)
    for at, column_of in enumerate((high[:8], high[8:], low[:8], low[8:])):
        stats = jnp.where(lane8 == at, column_of, stats)
    b_query[kv, pl.ds(0, SEQS)] = part[:, :128].astype(BF16)
    b_query[kv, pl.ds(SEQS, 8)] = stats.astype(BF16)
    send(2, b_query, kv, kv_peers)
    b_fresh[kv, pl.ds(0, SEQS)] = part[:, 128:256].astype(BF16)
    b_fresh[kv, pl.ds(SEQS, SEQS)] = part[:, 256:].astype(BF16)
    send(3, b_fresh, kv, kv_peers)
    settle(b_query, recv_sem.at[2])
    total = added(b_query)
    stats = total[SEQS:]
    squares = [
        jnp.sum(jnp.where((lane8 == at) | (lane8 == at + 2), stats, 0.0), axis=1, keepdims=True)
        for at in range(2)
    ]
    scale = lax.rsqrt(jnp.concatenate(squares, axis=0) / D + EPSILON)

    def rotate(vectors):
        swapped = jnp.where(in_half, pltpu.roll(vectors, 96, 1), pltpu.roll(vectors, 32, 1))
        return rounded(vectors * cosine + swapped * sine)

    query = rotate(scale * total[:SEQS])

    scale_att = DK ** (-0.5)
    front = tile_lane < DK
    rows8 = row_of(small) % 8
    live_lane = kv * BLOCK + lane_of((SEQS, BLOCK))
    peaks, sums = [], []
    for g in range(2):
        mine = query[8 * g : 8 * g + 8]
        twice = jnp.concatenate([mine, mine], axis=0)
        both = jnp.where((row < 8) == front, twice, 0.0)
        lhs = jnp.concatenate([jnp.where(rows8 == b, both, 0.0).astype(BF16) for b in range(8)], axis=1)
        scores = jnp.dot(lhs, v_keys_t[pl.ds(g * BLOCK, BLOCK)], preferred_element_type=F32)
        lens_g = lens[8 * g : 8 * g + 8]
        lens_g = jnp.concatenate([lens_g, lens_g], axis=0)
        live = live_lane < jnp.concatenate([lens_g] * (BLOCK // 128), axis=1)
        scores = jnp.where(live, scores * scale_att, MASKED_SCORE)
        block_max = jnp.max(scores, axis=1, keepdims=True)
        weights = jnp.where(live, jnp.exp(scores - block_max), 0.0)
        sums.append(jnp.sum(weights, axis=1, keepdims=True))
        peaks.append(block_max)
        weights = weights.astype(BF16)
        mixed = jnp.zeros(small, F32)
        for pair in range(4):
            b = 8 * g + 2 * pair
            rhs = jnp.concatenate([v_values[b + k] for k in range(2)], axis=1)
            product = jnp.dot(weights, rhs, preferred_element_type=F32)
            for k in range(2):
                mixed = jnp.where(rows8 == 2 * pair + k, product[:, k * DV : (k + 1) * DV], mixed)
        b_attn[kv, pl.ds(SEQS * g, SEQS)] = mixed.astype(BF16)

    wide = (2 * SEQS, 128)
    diagonal = lane_of(wide) % 32 == row_of(wide)

    def laid(columns):
        return jnp.sum(jnp.where(diagonal, jnp.concatenate(columns, axis=0), 0.0), axis=0, keepdims=True)

    peak, weight = laid(peaks), laid(sums)
    peak_high = rounded(peak)
    peak_mid = rounded(peak - peak_high)
    weight_high = rounded(weight)
    tile = jnp.zeros((8, 128), F32)
    row8 = row_of((8, 128))
    terms = (peak_high, peak_mid, peak - peak_high - peak_mid, weight_high, weight - weight_high)
    for at, term in enumerate(terms):
        tile = jnp.where(row8 == at, term, tile)
    b_attn[kv, pl.ds(2 * SEQS, 8)] = tile.astype(BF16)
    send(4, b_attn, kv, kv_peers)

    settle(b_fresh, recv_sem.at[3])
    total = added(b_fresh)
    key_new = rotate(scale * total[:SEQS])
    value_new = scale * total[SEQS:]
    product = query * key_new * scale_att
    own = [jnp.sum(jnp.where(f, product, 0.0), axis=1, keepdims=True) for f in (front, ~front)]
    own_score = laid([own[k % 2][8 * (k // 2) : 8 * (k // 2) + 8] for k in range(4)])
    fresh_rows = [value_new[8 * (k // 2) : 8 * (k // 2) + 8] for k in range(4)]
    fresh_rows = jnp.concatenate(fresh_rows + [jnp.zeros((96, 128), F32)], axis=0).astype(BF16)

    settle(b_attn, recv_sem.at[4])
    part_of = lane_of((8, 128)) // 32
    block_peaks, block_sums = [], []
    for q in range(4):
        tile = b_attn[4 * q, pl.ds(2 * SEQS, 8)].astype(F32)
        for k in range(1, 4):
            tile = jnp.where(part_of == k, b_attn[4 * q + k, pl.ds(2 * SEQS, 8)].astype(F32), tile)
        block_peaks.append(tile[0:1] + tile[1:2] + tile[2:3])
        block_sums.append(tile[3:4] + tile[4:5])

    def around(value, combine):
        return functools.reduce(combine, [pltpu.roll(value, 32 * k, 1) for k in range(1, 4)], value)

    peak = jnp.maximum(around(functools.reduce(jnp.maximum, block_peaks), jnp.maximum), own_score)
    shares = [jnp.exp(p - peak) for p in block_peaks]
    fresh = jnp.exp(own_score - peak)
    weighted = [share * s for share, s in zip(shares, block_sums)]
    inverse = 1.0 / (around(functools.reduce(jnp.add, weighted), jnp.add) + fresh)
    factors = [jnp.where(diagonal, share * inverse, 0.0) for share in shares]
    factors.append(jnp.where(lane_of(wide) == row_of(wide), fresh * inverse, 0.0))
    factors = jnp.concatenate(factors, axis=1)
    high = factors.astype(BF16)
    low = (factors - high.astype(F32)).astype(BF16)
    blocks = [b_attn[i, pl.ds(0, 2 * SEQS)] for i in range(GROUP)]
    blocks = jnp.concatenate(blocks + [fresh_rows], axis=0)
    mixed = jnp.dot(jnp.concatenate([high, low], axis=0), blocks, preferred_element_type=F32)
    mixed = mixed[: 2 * SEQS] + mixed[2 * SEQS :]
    heads = [mixed[16 * g : 16 * g + 8] - lambdas[0] * mixed[16 * g + 8 : 16 * g + 16] for g in range(2)]
    heads = jnp.concatenate(heads, axis=0)
    spread = jnp.sum(heads * heads, axis=1, keepdims=True) / DV
    normed = heads * lax.rsqrt(spread + EPSILON) * gain_row(2) * OUTPUT_KEEP
    b_proj[tp] = jnp.dot(normed.astype(BF16), v_out[...], preferred_element_type=F32).astype(BF16)
    send(5, b_proj, tp, tp_peers)
    settle(b_proj, recv_sem.at[5])
    second = rounded(first + added(b_proj))

    mix_partial(second, gain_row(3), 1, b_mix2)
    send(6, b_mix2, kv, kv_peers)
    settle(b_mix2, recv_sem.at[6])
    hidden = mix_hidden(b_mix2)
    b_down2[tp] = jnp.dot(hidden, v_down[1], preferred_element_type=F32).astype(BF16)
    send(7, b_down2, tp, tp_peers)
    settle(b_down2, recv_sem.at[7])
    v_result[...] = (second + 0.5 * added(b_down2)).astype(BF16)

    finished = fetch(v_result, out)
    sent = (b_mix1, b_down1, b_query, b_fresh, b_attn, b_proj, b_mix2, b_down2)
    for phase, buf in enumerate(sent):
        settle(buf, send_sem.at[phase])
    finished.wait()


def local(
    tokens,
    lengths,
    cache_keys,
    cache_values,
    lambdas,
    head_gain,
    attn_gain,
    w_query,
    w_key,
    w_value,
    w_out,
    first_gain,
    first_gate,
    first_up,
    first_down,
    second_gain,
    second_gate,
    second_up,
    second_down,
):
    inv_freq = (ROTARY_BASE ** (-(np.arange(128) % 32) / 32.0)).astype(np.float32)
    flat = (SEQS, BLOCK, DV)
    operands = (
        lengths,
        lambdas,
        jnp.asarray(inv_freq).reshape(1, 128),
        tokens,
        cache_keys.reshape(flat),
        cache_values.reshape(flat),
        head_gain.reshape(1, 128),
        attn_gain.reshape(1, 128),
        w_query,
        w_key,
        w_value,
        w_out,
        first_gain.reshape(1, 128),
        first_gate.T,
        first_up.T,
        first_down,
        second_gain.reshape(1, 128),
        second_gate.T,
        second_up.T,
        second_down,
    )
    hbm = pl.BlockSpec(memory_space=pltpu.HBM)
    return pl.pallas_call(
        kernel,
        name="layer",
        out_shape=jax.ShapeDtypeStruct((SEQS, 128), BF16),
        in_specs=[hbm, pl.BlockSpec(memory_space=pltpu.SMEM)] + [hbm] * (len(operands) - 2),
        out_specs=hbm,
        scratch_shapes=[
            pltpu.VMEM((SEQS, 128), BF16),
            pltpu.VMEM((1, 128), F32),
            pltpu.VMEM((4, 1, 128), BF16),
            pltpu.VMEM((2, 2 * WIDE, 128), BF16),
            pltpu.VMEM((2, WIDE, 128), BF16),
            pltpu.VMEM((128, 384), BF16),
            pltpu.VMEM((128, 128), BF16),
            pltpu.VMEM(flat, BF16),
            pltpu.VMEM(flat, BF16),
            pltpu.VMEM((SEQS * 128, BLOCK), BF16),
            pltpu.VMEM((SEQS, 128), BF16),
            pltpu.SMEM((SEQS,), jnp.int32),
            pltpu.VMEM((GROUP, SEQS, 2 * WIDE), BF16),
            pltpu.VMEM((GROUP, SEQS, 128), BF16),
            pltpu.VMEM((GROUP, SEQS + 8, 128), BF16),
            pltpu.VMEM((GROUP, 2 * SEQS, 128), BF16),
            pltpu.VMEM((GROUP, 2 * SEQS + 8, 128), BF16),
            pltpu.VMEM((GROUP, SEQS, 128), BF16),
            pltpu.VMEM((GROUP, SEQS, 2 * WIDE), BF16),
            pltpu.VMEM((GROUP, SEQS, 128), BF16),
            pltpu.SemaphoreType.DMA((20,)),
            pltpu.SemaphoreType.DMA((8,)),
            pltpu.SemaphoreType.DMA((8,)),
        ],
        compiler_params=pltpu.CompilerParams(
            collective_id=0, has_side_effects=True, vmem_limit_bytes=67_043_328
        ),
    )(*operands)


def solution(mesh):
    placed = (
        P(None, "kv"),
        P(),
        P(None, "kv", "tp", None),
        P(None, "kv", "tp", None),
        P("tp"),
        P(),
        P("kv"),
        P("kv", "tp"),
        P("kv", "tp"),
        P("kv", "tp"),
        P("tp", "kv"),
        P("kv"),
        P("kv", "tp"),
        P("kv", "tp"),
        P("tp", "kv"),
        P("kv"),
        P("kv", "tp"),
        P("kv", "tp"),
        P("tp", "kv"),
    )
    return jax.shard_map(
        local, mesh=mesh, in_specs=placed, out_specs=P(None, "kv"), check_vma=False
    )
```

time: 55.7 us -> 53.9 us (0.968)
  Pallas kernels: 53.7 us -> 51.8 us
    pallas_call x1, Pallas kernels: 53.7 us -> 51.8 us  [local(): pl.pallas_call(kernel, name='layer', out_shape=jax.ShapeDtypeStruct((SEQS...]
where the time goes in v2:
time: 53.9 us; the launch traced here: 53.8 us
  Pallas kernels  51.8 us (96%)
  local copies, waits for them, and re-layouts  1.28 us (2%)
  between operations  0.66 us (1%)
    pallas_call x1, Pallas kernels, local(): pl.pallas_call(kernel, name='layer', out_shape=jax.ShapeDtypeStruct((SEQS...  51.8 us
    unnamed x1, local copies, waits for them, and re-layouts  1.28 us

profile of v2, /device:TPU:1, one launch (start us, length us, event | category | flops | bytes accessed | tf_op | source)
XLA Modules:
  0.0 53.8 jit_solution(9166335348568066647)
XLA Ops:
  0.7 51.8 %layer.1 = bf16[16,128]{1,0:T(8,128)(2,1)} custom-call(s32[16]{0:T(128)} %lengths.1, f32[1]{0:T(128)S(6)} %copy.22.lambdas, f32[1,128]{1,0:T(1,128)} %constant.6.inv_freq, bf16[16,128]{1,0:T(8,128)(2,1)} %tokens.1, bf16[16,1024,128]{2,1,0:T(8,128)(2,1)} %bitcast.10, bf16[16,1024,128]{2,1,0:T(8,128)(2,1)} %bitcast.11, bf16[1,128]{1,0:T(2,128)(2,1)} %bitcast.16, ...), custom_call_target="tpu_custom_call" | custom-call | tf_op jit(solution)/shard_map/layer/pallas_call | solution.py:416
  52.5 1.3 %copy.23 = bf16[16,128]{1,0:T(8,128)(2,1)} copy(bf16[16,128]{1,0:T(8,128)(2,1)} %layer.1) | data formatting | bytes 8192
